TPU v7x, 512 devices: a whole 4x4x16 slice. The times are simulated.
512 devices in a mesh: ep: 32 (over z, core), tp: 16 (over y, x).
Axes of the slice: x: 4, y: 4, z: 16, core: 2. Of those that a mesh axis runs over, the one named last changes fastest.
Arguments:
- tokens: bfloat16 [8192, 2048], P('ep', 'tp'), may hold values from -800 to 800
- norm_gain: bfloat16 [2048], P('tp'), may hold values from 0.099609375 to 1.8984375
- w_gate: bfloat16 [32, 2048, 6144], P('ep', None, 'tp'), may hold values from -0.125 to 0.125
- w_up: bfloat16 [32, 2048, 6144], P('ep', None, 'tp'), may hold values from -0.125 to 0.125
- w_down: bfloat16 [32, 6144, 2048], P('ep', 'tp'), may hold values from -1.2757759 to 1.2757759
- routes: int32 [8192, 2], P('ep'), may hold values from 0 to 31, all different within a row; in each aligned block of 256 rows (0 to 255, 256 to 511, ...) at most 32 rows name the same one
- route_weights: float32 [8192, 2], P('ep'), may hold values from 0.1 to 1
- final_gain: bfloat16 [2048], P('tp'), may hold values from 0.099609375 to 1.8984375
Outputs:
- mixed_out: bfloat16 [8192, 2048], P('ep', 'tp')
Inputs may be any that keep to these rules, and one draw needn't show every extreme that they name: `routes`: A token's 2 experts differ. Among the tokens of one index of ep (aligned blocks of 256 rows), no expert is named by more than 32 tokens, a bound that some block reaches.
All inputs are finite; a program needn't handle non-finite values.
Results may differ from a plain program's by a relative error of at most 0.017.
Values may be sent and summed in bfloat16 or wider, within the bound.
A program may use at most 64 MiB of HBM per device.

v0:
```python
import jax
import jax.numpy as jnp
from jax import lax
from jax.sharding import PartitionSpec as P

EPS = 1e-06


def from_everyone(shard, axis):
    copies = jnp.broadcast_to(shard, (lax.axis_size(axis), *shard.shape))
    return lax.all_to_all(copies, axis, split_axis=0, concat_axis=0, tiled=True)


def over_copies(shard, axis):
    return from_everyone(shard, axis).sum(axis=0)


def cut_along(shard, dim, length):
    before, after = (shard.shape[:dim], shard.shape[dim + 1 :])
    return jnp.moveaxis(shard.reshape(*before, length, -1, *after), dim, 0)


def summed_on_arrival(shard, axis, dim):
    length = lax.axis_size(axis)
    tiles = lax.all_to_all(cut_along(shard, dim, length), axis, 0, 0, tiled=True)
    return jnp.sum(tiles.astype(jnp.float32), axis=0)


def slot_targets(routes, experts, capacity):
    flat = routes.reshape(-1)
    onehot = (flat[:, None] == jnp.arange(experts, dtype=jnp.int32)[None, :]).astype(jnp.int32)
    before = jnp.cumsum(onehot, axis=0) - onehot
    slot = jnp.sum(before * onehot, axis=1)
    return flat * capacity + slot


def local(tokens, norm_gain, w_gate, w_up, w_down, routes, route_weights, final_gain):
    experts = lax.axis_size("ep")
    tok_rows = tokens.shape[0]
    share = tokens.shape[1]
    width = share * lax.axis_size("tp")
    topk = routes.shape[1]
    capacity = 2 * tok_rows * topk // experts
    wide = tokens.astype(jnp.float32)
    input_squares = over_copies(jnp.sum(wide * wide, axis=1), "tp")
    scale = lax.rsqrt(input_squares / width + EPS)
    normed = (wide * scale[:, None] * norm_gain.astype(jnp.float32)[None, :]).astype(jnp.bfloat16)
    target = slot_targets(routes, experts, capacity)
    sources = jnp.repeat(jnp.arange(tok_rows, dtype=jnp.int32), topk)
    gate_w = w_gate[0]
    up_w = w_up[0]
    down_w = w_down[0]
    outbox = jnp.zeros((experts * capacity, share), jnp.bfloat16).at[target].set(normed[sources])
    inbox = lax.all_to_all(outbox, "ep", split_axis=0, concat_axis=0, tiled=True)
    piece = lax.all_gather(inbox, "tp", axis=1, tiled=True)
    gate = jnp.dot(piece, gate_w, preferred_element_type=jnp.float32)
    up = jnp.dot(piece, up_w, preferred_element_type=jnp.float32)
    hidden = (jax.nn.silu(gate) * up).astype(jnp.bfloat16)
    sums = summed_on_arrival(
        lax.dot_general(
            down_w, hidden, (((0,), (1,)), ((), ())), preferred_element_type=jnp.float32
        ).astype(jnp.bfloat16),
        "tp",
        0,
    )
    returned = lax.all_to_all(
        sums.astype(jnp.bfloat16), "ep", split_axis=1, concat_axis=1, tiled=True
    )
    picked = jnp.take(returned, target, axis=1).reshape(returned.shape[0], tok_rows, topk)
    combined = jnp.einsum("dtk,tk->td", picked.astype(jnp.float32), route_weights)
    local_squares = jnp.sum(combined * combined, axis=1)
    total_squares = over_copies(local_squares, "tp")
    final_scale = lax.rsqrt(total_squares / width + EPS)
    return (combined * final_scale[:, None] * final_gain.astype(jnp.float32)[None, :]).astype(
        jnp.bfloat16
    )


def solution(mesh):
    in_specs = (
        P("ep", "tp"),
        P("tp"),
        P("ep", None, "tp"),
        P("ep", None, "tp"),
        P("ep", "tp", None),
        P("ep", None),
        P("ep", None),
        P("tp"),
    )
    out_specs = P("ep", "tp")
    return jax.shard_map(local, mesh=mesh, in_specs=in_specs, out_specs=out_specs, check_vma=False)
```

profile of v0, /device:TPU:1, one launch (start us, length us, event | category | flops | bytes accessed | tf_op | source)
XLA Modules:
  0.0 259.8 jit_solution(18186526171175588482)
XLA Ops:
  6.5 1.1 fusion.9
  7.6 0.6 broadcast_in_dim.31
  8.3 7.6 %all-to-all-start = ((f32[16,1,256]{2,1,0:T(1,128)}), f32[16,1,256]{2,1,0:T(1,128)S(1)}, u32[]{:S(2)}, u32[]{:S(2)}) async-start(f32[16,1,256]{2,1,0:T(1,128)} %broadcast_in_dim.31), calls=%async_computation | async-start | bytes 32768 | tf_op jit(solution)/shard_map/all_to_all | solution.py:11
  15.9 0.8 copy.31
  17.0 0.7 broadcast_multiply_fusion
  17.7 1.2 reduce-window.6
  19.7 0.7 convert_element_type.37
  20.4 1.9 all-to-all-done
  22.3 0.9 fusion.11
  23.3 3.1 %scatter_custom_fusion = bf16[1024,128]{1,0:T(8,128)(2,1)S(1)} fusion(s32[512]{0:T(512)S(1)} %bitcast.62, bf16[256,128]{1,0:T(8,128)(2,1)S(1)} %fusion.11, s32[1024]{0:T(1024)S(1)} %pad_clamp_fusion.1, bf16[]{:T(256)} %constant.34.clone.1), kind=kCustom, calls=%fused_computation.17 | custom fusion | bytes 262146 | tf_op jit(solution)/shard_map/scatter | solution.py:53
  26.3 39.5 %all_to_all.41 = bf16[32,32,128]{2,1,0:T(8,128)(2,1)} all-to-all(bf16[32,32,128]{2,1,0:T(8,128)(2,1)S(1)} %bitcast.57), channel_id=1, replica_groups=mesh['ep'=32,'tp'=16] {'ep'}, dimensions={0} | all-to-all | bytes 524288 | tf_op jit(solution)/shard_map/all_to_all | solution.py:54
  65.9 59.4 %all-gather.2.cloned.1.call-done = bf16[1024,2048]{1,0:T(8,128)(2,1)} async-done(((bf16[1024,128]{1,0:T(8,128)(2,1)}), bf16[1024,2048]{1,0:T(8,128)(2,1)}) %all-gather.2.cloned.1.call-update) | async-done | bytes 4194320 | tf_op jit(solution)/shard_map/all_gather | solution.py:55
  125.3 5.7 %fusion.3 = f32[1024,384]{1,0:T(8,128)} fusion(bf16[1024,2048]{1,0:T(8,128)(2,1)} %all-gather.2.cloned.1.call-done, bf16[1,2048,384]{2,1,0:T(8,128)(2,1)S(1)} %copy-done.3), kind=kOutput, calls=%fused_computation.8 | convolution fusion | flops 1610612736 | bytes 7340032 | tf_op jit(solution)/shard_map/dot_general | solution.py:56
  131.0 9.6 %convert_bitcast_fusion = bf16[128,16,8,128]{3,2,1,0:T(8,128)(2,1)} fusion(bf16[1,384,2048]{2,1,0:T(8,128)(2,1)S(1)} %copy-done, f32[1024,384]{1,0:T(8,128)} %fusion.3, bf16[1024,2048]{1,0:T(8,128)(2,1)} %all-gather.2.cloned.1.call-done, bf16[1,2048,384]{2,1,0:T(8,128)(2,1)} %param.11), kind=kOutput, calls=%fused_computation.4 | convolution fusion | flops 3225681920 | bytes 13107200 | tf_op jit(solution)/shard_map/dot_general | solution.py:60
  140.6 3.3 %copy.48 = bf16[128,16,8,128]{3,2,0,1:T(8,128)(2,1)S(1)} copy(bf16[128,16,8,128]{3,2,1,0:T(8,128)(2,1)} %convert_bitcast_fusion) | data formatting | bytes 8388608 | tf_op jit(solution)/shard_map/reshape | solution.py:20
  143.9 54.5 %all_to_all.42 = bf16[16,128,1024]{1,2,0:T(8,128)(2,1)} all-to-all(bf16[16,128,1024]{1,2,0:T(8,128)(2,1)S(1)} %bitcast.54), channel_id=1, replica_groups=mesh['ep'=32,'tp'=16] {'tp'}, dimensions={0} | all-to-all | bytes 8388608 | tf_op jit(solution)/shard_map/all_to_all | solution.py:25
  198.3 3.5 %reduce_sum.66 = bf16[128,1024]{0,1:T(8,128)(2,1)} reduce(bf16[16,128,1024]{1,2,0:T(8,128)(2,1)} %all_to_all.42, bf16[]{:T(256)} %constant.34.clone.1), dimensions={0}, to_apply=%region_6.7 | reduce | flops 1966080 | bytes 4456450 | tf_op jit(solution)/shard_map/reduce_sum | solution.py:26
  201.9 15.5 %all-to-all-start.3 = ((bf16[128,32,32]{0,2,1:T(8,128)(2,1)}), bf16[128,32,32]{0,2,1:T(8,128)(2,1)S(1)}, u32[]{:S(2)}, u32[]{:S(2)}) async-start(bf16[128,32,32]{0,2,1:T(8,128)(2,1)} %bitcast.10), calls=%async_computation.3 | async-start | bytes 524288 | tf_op jit(solution)/shard_map/all_to_all | solution.py:66
  218.0 21.6 %all-to-all-done.3 = bf16[128,32,32]{0,2,1:T(8,128)(2,1)S(1)} async-done(((bf16[128,32,32]{0,2,1:T(8,128)(2,1)}), bf16[128,32,32]{0,2,1:T(8,128)(2,1)S(1)}, u32[]{:S(2)}, u32[]{:S(2)}) %all-to-all-start.3) | async-done | bytes 262176 | tf_op jit(solution)/shard_map/all_to_all | solution.py:66
  239.7 1.3 gather_fusion
  241.6 0.6 broadcast_in_dim.34
  242.2 3.5 %all-to-all-start.4 = ((f32[16,1,256]{2,1,0:T(1,128)}), f32[16,1,256]{2,1,0:T(1,128)S(1)}, u32[]{:S(2)}, u32[]{:S(2)}) async-start(f32[16,1,256]{2,1,0:T(1,128)} %broadcast_in_dim.34), calls=%async_computation.4 | async-start | bytes 32768 | tf_op jit(solution)/shard_map/all_to_all | solution.py:11
  245.8 6.4 %all-to-all-done.4 = f32[16,1,256]{2,1,0:T(1,128)S(1)} async-done(((f32[16,1,256]{2,1,0:T(1,128)}), f32[16,1,256]{2,1,0:T(1,128)S(1)}, u32[]{:S(2)}, u32[]{:S(2)}) %all-to-all-start.4) | async-done | bytes 16416 | tf_op jit(solution)/shard_map/all_to_all | solution.py:11
  252.2 0.7 multiply_convert_fusion.1
  (39 shorter events, 2.5 us)
Async XLA Ops:
  6.5 124.5 %copy-start = (bf16[1,384,2048]{2,1,0:T(8,128)(2,1)S(1)}, bf16[1,384,2048]{2,1,0:T(8,128)(2,1)}, u32[]{:S(2)}) copy-start(bf16[1,384,2048]{2,1,0:T(8,128)(2,1)} %param.12) | copy-start | bytes 4718596
  6.5 118.7 %copy-start.3 = (bf16[1,2048,384]{2,1,0:T(8,128)(2,1)S(1)}, bf16[1,2048,384]{2,1,0:T(8,128)(2,1)}, u32[]{:S(2)}) copy-start(bf16[1,2048,384]{2,1,0:T(8,128)(2,1)} %param.10) | copy-start | bytes 4718596
  8.3 14.0 %all-to-all-start = ((f32[16,1,256]{2,1,0:T(1,128)}), f32[16,1,256]{2,1,0:T(1,128)S(1)}, u32[]{:S(2)}, u32[]{:S(2)}) async-start(f32[16,1,256]{2,1,0:T(1,128)} %broadcast_in_dim.31), calls=%async_computation | async-start | bytes 32768 | tf_op jit(solution)/shard_map/all_to_all | solution.py:11
  15.8 109.4 %all-gather.2.cloned.1.call-start = ((), (), s32[]{:S(2)}) async-start(), calls=%async_computation.5 | async-start | bytes 4456448 | tf_op jit(solution)/shard_map/all_gather | solution.py:55
  198.3 19.3 %copy-start.1 = (s32[256,2]{0,1:T(2,128)S(1)}, s32[256,2]{0,1:T(2,128)}, u32[]{:S(2)}) copy-start(s32[256,2]{0,1:T(2,128)} %param.13) | copy-start | bytes 6148
  198.3 19.5 %copy-start.2 = (f32[256,2]{0,1:T(2,128)S(1)}, f32[256,2]{0,1:T(2,128)}, u32[]{:S(2)}) copy-start(f32[256,2]{0,1:T(2,128)} %param.14) | copy-start | bytes 6148
  201.9 37.8 %all-to-all-start.3 = ((bf16[128,32,32]{0,2,1:T(8,128)(2,1)}), bf16[128,32,32]{0,2,1:T(8,128)(2,1)S(1)}, u32[]{:S(2)}, u32[]{:S(2)}) async-start(bf16[128,32,32]{0,2,1:T(8,128)(2,1)} %bitcast.10), calls=%async_computation.3 | async-start | bytes 524288 | tf_op jit(solution)/shard_map/all_to_all | solution.py:66
  239.7 6.1 %copy-start.4 = (bf16[128]{0:T(256)(128)(2,1)S(1)}, bf16[128]{0:T(256)(128)(2,1)}, u32[]{:S(2)}) copy-start(bf16[128]{0:T(256)(128)(2,1)} %param.15) | copy-start | bytes 772
  242.2 9.9 %all-to-all-start.4 = ((f32[16,1,256]{2,1,0:T(1,128)}), f32[16,1,256]{2,1,0:T(1,128)S(1)}, u32[]{:S(2)}, u32[]{:S(2)}) async-start(f32[16,1,256]{2,1,0:T(1,128)} %broadcast_in_dim.34), calls=%async_computation.4 | async-start | bytes 32768 | tf_op jit(solution)/shard_map/all_to_all | solution.py:11
Sparse Core Ops, SparseCore 0:
  66.0 59.2 all-gather.1
where the time goes:
time: 260 us
  blocking collectives  94 us (36%)
  waiting for transfers between devices  89.3 us (34%)
  starting transfers between devices  26.6 us (10%)
  matrix products  15.8 us (6%)
  between operations  13.6 us (5%)
  local copies, waits for them, and re-layouts  11.2 us (4%)
  other arithmetic  9.22 us (4%)
    all_gather x1, waiting for transfers between devices, local(): piece = lax.all_gather(inbox, 'tp', axis=1, tiled=True)  59.4 us
    all_to_all x1, blocking collectives, summed_on_arrival(): lax.all_to_all(cut_along(shard, dim, length), axis, 0, 0, tiled=True)  54.5 us
    all_to_all x1, blocking collectives, local(): lax.all_to_all(outbox, 'ep', split_axis=0, concat_axis=0, tiled=True)  39.5 us
    all_to_all x1, waiting for transfers between devices, local(): lax.all_to_all(sums.astype(jnp.bfloat16), 'ep', split_axis=1, concat_axis...  21.6 us
    all_to_all x1, starting transfers between devices, local(): lax.all_to_all(sums.astype(jnp.bfloat16), 'ep', split_axis=1, concat_axis...  15.5 us
    all_to_all x2, starting transfers between devices, from_everyone(): return lax.all_to_all(copies, axis, split_axis=0, concat_axis=0, tiled=True)  11.1 us
    dot_general x1, matrix products, local(): lax.dot_general(down_w, hidden, (((0,), (1,)), ((), ())), preferred_eleme...  9.6 us
    all_to_all x2, waiting for transfers between devices, from_everyone(): return lax.all_to_all(copies, axis, split_axis=0, concat_axis=0, tiled=True)  8.25 us
  transfers between devices with their start and end apart: 4, of which 4 were waited for; matrix products, arithmetic and copies ran while one was open for 2% of the time, Pallas kernels for 0%

commit v1 on v0

--- a/solution.py
+++ b/solution.py
@@ -52,7 +52,9 @@
     down_w = w_down[0]
     outbox = jnp.zeros((experts * capacity, share), jnp.bfloat16).at[target].set(normed[sources])
     inbox = lax.all_to_all(outbox, "ep", split_axis=0, concat_axis=0, tiled=True)
-    piece = lax.all_gather(inbox, "tp", axis=1, tiled=True)
+    piece = jnp.concatenate(
+        lax.all_to_all(jnp.stack([inbox] * lax.axis_size("tp")), "tp", 0, 0), axis=1
+    )
     gate = jnp.dot(piece, gate_w, preferred_element_type=jnp.float32)
     up = jnp.dot(piece, up_w, preferred_element_type=jnp.float32)
     hidden = (jax.nn.silu(gate) * up).astype(jnp.bfloat16)

time: 260 us -> 230 us (0.88)
  waiting for transfers between devices: 89.3 us -> 29.9 us
  blocking collectives: 94 us -> 146 us
  between operations: 13.6 us -> 0.22 us
  starting transfers between devices: 26.6 us -> 18.4 us
  matrix products: 15.8 us -> 12 us
  local copies, waits for them, and re-layouts: 11.2 us -> 13.8 us
    all_gather x1 -> x0, waiting for transfers between devices: 59.4 us -> none  [local(): piece = lax.all_gather(inbox, 'tp', axis=1, tiled=True)]
    all_to_all x0 -> x1, blocking collectives: none -> 53.5 us  [local(): lax.all_to_all(jnp.stack([inbox] * lax.axis_size('tp')), 'tp', 0, 0)]
    all_to_all x1, starting transfers between devices: 15.5 us -> 7.29 us  [local(): lax.all_to_all(sums.astype(jnp.bfloat16), 'ep', split_axis=1, concat_axis...]
  transfers between devices with their start and end apart: 4 -> 3, of which waited for: 4 -> 3; matrix products, arithmetic and copies ran while one was open for 2% -> 2% of each run, Pallas kernels for 0% -> 0%
where the time goes in v1:
time: 230 us
  blocking collectives  146 us (63%)
  waiting for transfers between devices  29.9 us (13%)
  starting transfers between devices  18.4 us (8%)
  local copies, waits for them, and re-layouts  13.8 us (6%)
  matrix products  12 us (5%)
  other arithmetic  9.19 us (4%)
    all_to_all x1, blocking collectives, local(): lax.all_to_all(jnp.stack([inbox] * lax.axis_size('tp')), 'tp', 0, 0)  53.5 us
    all_to_all x1, blocking collectives, summed_on_arrival(): lax.all_to_all(cut_along(shard, dim, length), axis, 0, 0, tiled=True)  53.1 us
    all_to_all x1, blocking collectives, local(): lax.all_to_all(outbox, 'ep', split_axis=0, concat_axis=0, tiled=True)  39.4 us
    all_to_all x1, waiting for transfers between devices, local(): lax.all_to_all(sums.astype(jnp.bfloat16), 'ep', split_axis=1, concat_axis...  21.6 us
    all_to_all x2, starting transfers between devices, from_everyone(): return lax.all_to_all(copies, axis, split_axis=0, concat_axis=0, tiled=True)  11.1 us
    all_to_all x2, waiting for transfers between devices, from_everyone(): return lax.all_to_all(copies, axis, split_axis=0, concat_axis=0, tiled=True)  8.3 us
    dot_general x1, matrix products, local(): lax.dot_general(down_w, hidden, (((0,), (1,)), ((), ())), preferred_eleme...  7.91 us
    all_to_all x1, starting transfers between devices, local(): lax.all_to_all(sums.astype(jnp.bfloat16), 'ep', split_axis=1, concat_axis...  7.29 us
  transfers between devices with their start and end apart: 3, of which 3 were waited for; matrix products, arithmetic and copies ran while one was open for 2% of the time, Pallas kernels for 0%

profile of v1, /device:TPU:1, one launch (start us, length us, event | category | flops | bytes accessed | tf_op | source)
XLA Modules:
  0.0 229.6 jit_solution(8643207585627709610)
XLA Ops:
  0.0 1.1 fusion.9
  1.7 7.6 %all-to-all-start = ((f32[16,1,256]{2,1,0:T(1,128)}), f32[16,1,256]{2,1,0:T(1,128)S(1)}, u32[]{:S(2)}, u32[]{:S(2)}) async-start(f32[16,1,256]{2,1,0:T(1,128)} %broadcast_in_dim.31), calls=%async_computation | async-start | bytes 32768 | tf_op jit(solution)/shard_map/all_to_all | solution.py:11
  9.3 0.8 copy.39
  10.4 0.7 broadcast_multiply_fusion
  11.1 1.2 reduce-window.6
  13.1 0.7 convert_element_type.37
  13.8 1.9 all-to-all-done
  15.8 0.9 fusion.11
  16.7 3.1 %scatter_custom_fusion = bf16[1024,128]{1,0:T(8,128)(2,1)S(1)} fusion(s32[512]{0:T(512)S(1)} %bitcast.67, bf16[256,128]{1,0:T(8,128)(2,1)S(1)} %fusion.11, s32[1024]{0:T(1024)S(1)} %pad_clamp_fusion.1, bf16[]{:T(256)} %constant.34.clone.1), kind=kCustom, calls=%fused_computation.17 | custom fusion | bytes 262146 | tf_op jit(solution)/shard_map/scatter | solution.py:53
  19.8 39.4 %all_to_all.43 = bf16[32,32,128]{2,1,0:T(8,128)(2,1)S(1)} all-to-all(bf16[32,32,128]{2,1,0:T(8,128)(2,1)S(1)} %bitcast.61), channel_id=1, replica_groups=mesh['ep'=32,'tp'=16] {'ep'}, dimensions={0} | all-to-all | bytes 524288 | tf_op jit(solution)/shard_map/all_to_all | solution.py:54
  59.9 53.5 %all_to_all.44 = bf16[16,1024,128]{1,2,0:T(8,128)(2,1)S(1)} all-to-all(bf16[16,1024,128]{1,2,0:T(8,128)(2,1)S(1)} %stack.5), channel_id=1, replica_groups=mesh['ep'=32,'tp'=16] {'tp'}, dimensions={0} | all-to-all | bytes 8388608 | tf_op jit(solution)/shard_map/all_to_all | solution.py:56
  113.4 1.9 copy-done.1
  115.4 3.6 %fusion.3 = f32[1024,384]{1,0:T(8,128)} fusion(bf16[1024,2048]{0,1:T(8,128)(2,1)S(1)} %bitcast.59, bf16[1,2048,384]{2,1,0:T(8,128)(2,1)S(1)} %copy-done.4), kind=kOutput, calls=%fused_computation.8 | convolution fusion | flops 1610612736 | bytes 7340032 | tf_op jit(solution)/shard_map/dot_general | solution.py:58
  119.0 7.9 %convert_bitcast_fusion = bf16[128,16,8,128]{3,2,1,0:T(8,128)(2,1)} fusion(bf16[1,384,2048]{2,1,0:T(8,128)(2,1)S(1)} %copy-done, f32[1024,384]{1,0:T(8,128)} %fusion.3, bf16[1024,2048]{0,1:T(8,128)(2,1)} %bitcast.60, bf16[1,2048,384]{2,1,0:T(8,128)(2,1)S(1)} %copy-done.5), kind=kOutput, calls=%fused_computation.4 | convolution fusion | flops 3225681920 | bytes 13107200 | tf_op jit(solution)/shard_map/dot_general | solution.py:62
  126.9 3.3 %copy.57 = bf16[128,16,8,128]{3,2,0,1:T(8,128)(2,1)S(1)} copy(bf16[128,16,8,128]{3,2,1,0:T(8,128)(2,1)} %convert_bitcast_fusion) | data formatting | bytes 8388608 | tf_op jit(solution)/shard_map/reshape | solution.py:20
  130.1 53.1 %all_to_all.45 = bf16[16,128,1024]{1,2,0:T(8,128)(2,1)} all-to-all(bf16[16,128,1024]{1,2,0:T(8,128)(2,1)S(1)} %bitcast.57), channel_id=1, replica_groups=mesh['ep'=32,'tp'=16] {'tp'}, dimensions={0} | all-to-all | bytes 8388608 | tf_op jit(solution)/shard_map/all_to_all | solution.py:25
  183.2 3.5 %reduce_sum.66 = bf16[128,1024]{0,1:T(8,128)(2,1)} reduce(bf16[16,128,1024]{1,2,0:T(8,128)(2,1)} %all_to_all.45, bf16[]{:T(256)} %constant.34.clone.1), dimensions={0}, to_apply=%region_6.7 | reduce | flops 1966080 | bytes 4456450 | tf_op jit(solution)/shard_map/reduce_sum | solution.py:26
  186.8 7.3 %all-to-all-start.4 = ((bf16[128,32,32]{0,2,1:T(8,128)(2,1)}), bf16[128,32,32]{0,2,1:T(8,128)(2,1)S(1)}, u32[]{:S(2)}, u32[]{:S(2)}) async-start(bf16[128,32,32]{0,2,1:T(8,128)(2,1)} %bitcast.13), calls=%async_computation.4 | async-start | bytes 524288 | tf_op jit(solution)/shard_map/all_to_all | solution.py:68
  194.7 21.6 %all-to-all-done.4 = bf16[128,32,32]{0,2,1:T(8,128)(2,1)S(1)} async-done(((bf16[128,32,32]{0,2,1:T(8,128)(2,1)}), bf16[128,32,32]{0,2,1:T(8,128)(2,1)S(1)}, u32[]{:S(2)}, u32[]{:S(2)}) %all-to-all-start.4) | async-done | bytes 262176 | tf_op jit(solution)/shard_map/all_to_all | solution.py:68
  216.3 1.3 gather_fusion
  218.3 0.6 broadcast_in_dim.34
  218.9 3.5 %all-to-all-start.5 = ((f32[16,1,256]{2,1,0:T(1,128)}), f32[16,1,256]{2,1,0:T(1,128)S(1)}, u32[]{:S(2)}, u32[]{:S(2)}) async-start(f32[16,1,256]{2,1,0:T(1,128)} %broadcast_in_dim.34), calls=%async_computation.5 | async-start | bytes 32768 | tf_op jit(solution)/shard_map/all_to_all | solution.py:11
  222.4 6.4 %all-to-all-done.5 = f32[16,1,256]{2,1,0:T(1,128)S(1)} async-done(((f32[16,1,256]{2,1,0:T(1,128)}), f32[16,1,256]{2,1,0:T(1,128)S(1)}, u32[]{:S(2)}, u32[]{:S(2)}) %all-to-all-start.5) | async-done | bytes 16416 | tf_op jit(solution)/shard_map/all_to_all | solution.py:11
  228.8 0.7 multiply_convert_fusion.1
  (43 shorter events, 3.7 us)
Async XLA Ops:
  0.0 119.0 %copy-start = (bf16[1,384,2048]{2,1,0:T(8,128)(2,1)S(1)}, bf16[1,384,2048]{2,1,0:T(8,128)(2,1)}, u32[]{:S(2)}) copy-start(bf16[1,384,2048]{2,1,0:T(8,128)(2,1)} %param.12) | copy-start | bytes 4718596
  1.7 14.0 %all-to-all-start = ((f32[16,1,256]{2,1,0:T(1,128)}), f32[16,1,256]{2,1,0:T(1,128)S(1)}, u32[]{:S(2)}, u32[]{:S(2)}) async-start(f32[16,1,256]{2,1,0:T(1,128)} %broadcast_in_dim.31), calls=%async_computation | async-start | bytes 32768 | tf_op jit(solution)/shard_map/all_to_all | solution.py:11
  59.9 55.5 %copy-start.4 = (bf16[1,2048,384]{2,1,0:T(8,128)(2,1)S(1)}, bf16[1,2048,384]{2,1,0:T(8,128)(2,1)}, u32[]{:S(2)}) copy-start(bf16[1,2048,384]{2,1,0:T(8,128)(2,1)} %param.10) | copy-start | bytes 4718596
  113.4 1.9 copy-start.1
  115.4 3.6 %copy-start.5 = (bf16[1,2048,384]{2,1,0:T(8,128)(2,1)S(1)}, bf16[1,2048,384]{2,1,0:T(8,128)(2,1)}, u32[]{:S(2)}) copy-start(bf16[1,2048,384]{2,1,0:T(8,128)(2,1)} %param.11) | copy-start | bytes 4718596
  183.2 11.0 %copy-start.2 = (s32[256,2]{0,1:T(2,128)S(1)}, s32[256,2]{0,1:T(2,128)}, u32[]{:S(2)}) copy-start(s32[256,2]{0,1:T(2,128)} %param.13) | copy-start | bytes 6148
  183.2 11.3 %copy-start.3 = (f32[256,2]{0,1:T(2,128)S(1)}, f32[256,2]{0,1:T(2,128)}, u32[]{:S(2)}) copy-start(f32[256,2]{0,1:T(2,128)} %param.14) | copy-start | bytes 6148
  186.8 29.6 %all-to-all-start.4 = ((bf16[128,32,32]{0,2,1:T(8,128)(2,1)}), bf16[128,32,32]{0,2,1:T(8,128)(2,1)S(1)}, u32[]{:S(2)}, u32[]{:S(2)}) async-start(bf16[128,32,32]{0,2,1:T(8,128)(2,1)} %bitcast.13), calls=%async_computation.4 | async-start | bytes 524288 | tf_op jit(solution)/shard_map/all_to_all | solution.py:68
  216.3 6.1 %copy-start.6 = (bf16[128]{0:T(256)(128)(2,1)S(1)}, bf16[128]{0:T(256)(128)(2,1)}, u32[]{:S(2)}) copy-start(bf16[128]{0:T(256)(128)(2,1)} %param.15) | copy-start | bytes 772
  218.9 9.9 %all-to-all-start.5 = ((f32[16,1,256]{2,1,0:T(1,128)}), f32[16,1,256]{2,1,0:T(1,128)S(1)}, u32[]{:S(2)}, u32[]{:S(2)}) async-start(f32[16,1,256]{2,1,0:T(1,128)} %broadcast_in_dim.34), calls=%async_computation.5 | async-start | bytes 32768 | tf_op jit(solution)/shard_map/all_to_all | solution.py:11
